TPU v7x, 512 devices: a 8x2x16 block of a 8x16x16 slice. The times are simulated.
512 devices in a mesh: grp: 2 (over y), sp: 16 (over z), tp: 16 (over x, core).
Axes of the slice: x: 8, y: 2, z: 16, core: 2. Of those that a mesh axis runs over, the one named last changes fastest.
The devices are a block of a 8x16x16 slice.
Arguments:
- target: bfloat16 [4096, 2048], P(('grp', 'sp', 'tp')), parts along dimension 0, may hold values from -6 to 6
- source: bfloat16 [32768, 2048], P(('grp', 'sp', 'tp')), parts along dimension 0, may hold values from -6 to 6
- norm_gain: float32 [2048], replicated, may hold values from 0.1 to 1.9
- query_weight: bfloat16 [2048, 2048], P(None, 'tp'), may hold values from -0.125 to 0.125
- key_weight: bfloat16 [2048, 256], replicated, may hold values from -0.125 to 0.125
- value_weight: bfloat16 [2048, 256], replicated, may hold values from -0.125 to 0.125
- output_weight: bfloat16 [2048, 2048], P('tp'), may hold values from -0.125 to 0.125
- saved_out: bfloat16 [4096, 2048], P(('grp', 'sp'), 'tp'), parts along dimension 0, may hold values from -3 to 3
- log_shift: float32 [16, 4096], P('tp', ('grp', 'sp')), parts along dimension 1, may hold values from 0 to 2
- out_grad: bfloat16 [4096, 2048], P(('grp', 'sp', 'tp')), parts along dimension 0, may hold values from -48 to 48
Outputs:
- target_grad: float32 [4096, 2048], P(('grp', 'sp', 'tp')), parts along dimension 0
- source_grad: float32 [32768, 2048], P(('grp', 'sp', 'tp')), parts along dimension 0
- query_weight_grad: float32 [4096, 2048], P(('grp', 'sp'), 'tp'), parts along dimension 0
There are 2 independent parts, one for each index of `grp`. A program takes and returns all parts, laid end to end along the dimension named above; an argument that names none is the same for every part. Nothing has to cross between parts.
All inputs are finite; a program needn't handle non-finite values.
Results may differ from a plain program's by a relative error of at most 0.02.
Values may be sent and summed in bfloat16 or wider, within the bound.
A program may use at most 64 MiB of HBM per device.

v0:
```python
import jax
import jax.numpy as jnp
from jax import lax
from jax.sharding import PartitionSpec as P

HEADS = 16
HEAD_DIM = 128
KV_HEADS = 2


def cut_along(array, dim, count):
    dims = array.shape
    blocks = array.reshape(*dims[:dim], count, dims[dim] // count, *dims[dim + 1 :])
    return jnp.moveaxis(blocks, dim, 0)


def summed_on_arrival(array, axis, dim):
    blocks = cut_along(array, dim, lax.axis_size(axis))
    arrived = lax.all_to_all(blocks, axis, split_axis=0, concat_axis=0, tiled=True)
    return arrived.astype(jnp.float32).sum(axis=0)


def attend(query_heads, back_heads, shift_cols, drop_cols, key_rows, values, offset):
    factor = HEAD_DIM ** (-0.5)
    scores = (
        jnp.einsum("nhd,md->hnm", query_heads, key_rows, preferred_element_type=jnp.float32)
        * factor
    )
    prob = jnp.exp(scores - shift_cols.T[:, :, None] - offset)
    prob_grad = jnp.einsum("nhd,md->hnm", back_heads, values, preferred_element_type=jnp.float32)
    score_grad = (prob * (prob_grad - drop_cols.T[:, :, None]) * factor).astype(jnp.bfloat16)
    return (prob.astype(jnp.bfloat16), score_grad)


def shards(
    target,
    source,
    norm_gain,
    query_weight,
    key_weight,
    value_weight,
    output_weight,
    saved_out,
    log_shift,
    out_grad,
):
    tp_count = lax.axis_size("tp")
    sp_count = lax.axis_size("sp")
    local_heads = query_weight.shape[1] // HEAD_DIM
    head_width = local_heads * HEAD_DIM
    model_width = target.shape[1]
    group_size = HEADS // KV_HEADS
    pair_index = lax.axis_index("tp") * local_heads // group_size
    offset = jnp.log(jnp.float32(source.shape[0] * tp_count * sp_count))
    target_wide = target.astype(jnp.float32)
    root_mean = jnp.sqrt(jnp.mean(target_wide * target_wide, axis=1, keepdims=True) + 1e-06)
    normed = (target_wide / root_mean * norm_gain).astype(jnp.bfloat16)
    joined = jnp.concatenate([normed, out_grad], axis=1)
    portion = lax.all_gather(joined, "tp", axis=0, tiled=True)
    normed_part = portion[:, :model_width]
    query_part = jnp.dot(normed_part, query_weight, preferred_element_type=jnp.float32).astype(
        jnp.bfloat16
    )
    back_part = lax.dot_general(
        portion[:, model_width:],
        output_weight,
        (((1,), (1,)), ((), ())),
        preferred_element_type=jnp.float32,
    ).astype(jnp.bfloat16)
    gathered = jnp.concatenate([query_part, back_part, normed_part], axis=1)
    queries = gathered[:, :head_width]
    out_back = gathered[:, head_width : 2 * head_width]
    normed_all = gathered[:, 2 * head_width :]
    tgt_local = queries.shape[0]
    key_cols = lax.dynamic_slice_in_dim(key_weight, pair_index * HEAD_DIM, HEAD_DIM, 1)
    value_cols = lax.dynamic_slice_in_dim(value_weight, pair_index * HEAD_DIM, HEAD_DIM, 1)
    both_cols = jnp.concatenate([key_cols, value_cols], axis=1)
    paired = jnp.dot(
        lax.all_gather(source, "tp", axis=0, tiled=True),
        both_cols,
        preferred_element_type=jnp.float32,
    ).astype(jnp.bfloat16)
    key_rows = paired[:, :HEAD_DIM]
    values = paired[:, HEAD_DIM:]
    products = out_back.astype(jnp.float32) * saved_out.astype(jnp.float32)
    drop_cols = jnp.sum(products.reshape(tgt_local, local_heads, HEAD_DIM), axis=2)
    shift_cols = log_shift.T
    portion = (
        lax.all_gather(queries, "sp", axis=0, tiled=True),
        lax.all_gather(out_back, "sp", axis=0, tiled=True),
        lax.all_gather(shift_cols.astype(jnp.bfloat16), "sp", axis=0, tiled=True).astype(
            jnp.float32
        ),
        lax.all_gather(drop_cols.astype(jnp.bfloat16), "sp", axis=0, tiled=True).astype(
            jnp.float32
        ),
    )
    query_part, back_part, shift_part, drop_part = portion
    count_rows = query_part.shape[0]
    query_three = query_part.reshape(count_rows, local_heads, HEAD_DIM)
    back_three = back_part.reshape(count_rows, local_heads, HEAD_DIM)
    prob_low, score_grad = attend(
        query_three, back_three, shift_part, drop_part, key_rows, values, offset
    )
    key_sum = jnp.einsum("hnm,nhd->md", score_grad, query_three, preferred_element_type=jnp.float32)
    value_sum = jnp.einsum("hnm,nhd->md", prob_low, back_three, preferred_element_type=jnp.float32)
    key_sum, value_sum, score_grad = (key_sum, value_sum, score_grad)
    count_rows = portion[0].shape[0]
    added = jnp.einsum(
        "hnm,md->nhd", score_grad, key_rows, preferred_element_type=jnp.float32
    ).reshape(count_rows, head_width)
    query_sum = summed_on_arrival(added.astype(jnp.bfloat16), "sp", 0)
    query_grad = query_sum.astype(jnp.bfloat16)
    stacked = jnp.concatenate([key_sum, value_sum], axis=1)[:, None, :]
    received = lax.all_to_all(
        stacked.astype(jnp.bfloat16), "tp", split_axis=0, concat_axis=1, tiled=True
    ).astype(stacked.dtype)
    own_rows = received.shape[0]
    grouped = jnp.sum(
        received.reshape(own_rows, KV_HEADS, tp_count // KV_HEADS, 2 * HEAD_DIM), axis=2
    )
    key_grad = grouped[:, :, :HEAD_DIM].reshape(own_rows, KV_HEADS * HEAD_DIM).astype(jnp.bfloat16)
    value_grad = (
        grouped[:, :, HEAD_DIM:].reshape(own_rows, KV_HEADS * HEAD_DIM).astype(jnp.bfloat16)
    )
    contract = (((1,), (1,)), ((), ()))
    source_grad = lax.dot_general(
        key_grad, key_weight, contract, preferred_element_type=jnp.float32
    ) + lax.dot_general(value_grad, value_weight, contract, preferred_element_type=jnp.float32)
    picked = query_grad
    normed_grad = summed_on_arrival(
        lax.dot_general(picked, query_weight, contract, preferred_element_type=jnp.float32).astype(
            jnp.bfloat16
        ),
        "tp",
        0,
    )
    scaled_grad = normed_grad * norm_gain
    target_grad = (
        scaled_grad / root_mean
        - target_wide * jnp.mean(scaled_grad * target_wide, axis=1, keepdims=True) / root_mean**3
    )
    picked = normed_all
    query_weight_grad = summed_on_arrival(
        lax.dot_general(
            picked, query_grad, (((0,), (0,)), ((), ())), preferred_element_type=jnp.float32
        ).astype(jnp.bfloat16),
        "sp",
        0,
    )
    return (target_grad, source_grad, query_weight_grad)


def solution(mesh):
    return jax.shard_map(
        shards,
        mesh=mesh,
        in_specs=(
            P(("grp", "sp", "tp"), None),
            P(("grp", "sp", "tp"), None),
            P(),
            P(None, "tp"),
            P(),
            P(),
            P("tp", None),
            P(("grp", "sp"), "tp"),
            P("tp", ("grp", "sp")),
            P(("grp", "sp", "tp"), None),
        ),
        out_specs=(
            P(("grp", "sp", "tp"), None),
            P(("grp", "sp", "tp"), None),
            P(("grp", "sp"), "tp"),
        ),
        check_vma=False,
    )
```

profile of v0, /device:TPU:65, one launch (start us, length us, event | category | flops | bytes accessed | tf_op | source)
XLA Modules:
  0.0 308.8 jit_solution(2163993728256108957)
XLA Ops:
  7.3 0.9 fusion.43
  9.1 1.4 pad_maximum_fusion.1
  12.9 61.8 %all-gather = bf16[1,2048]{1,0:T(2,128)(2,1)S(1)} all-gather(bf16[1,128]{1,0:T(2,128)(2,1)S(1)} %convert_element_type.126), channel_id=2, replica_groups=mesh['grp'=2,'sp'=16,'tp'=16] {'sp'}, dimensions={1}, use_global_device_ids=true | all-gather | bytes 4352 | tf_op jit(solution)/shard_map/all_gather | solution.py:91
  74.7 1.3 constant_dynamic-slice_fusion
  76.0 14.3 %all-gather.8.cloned.1.call-done = bf16[128,4096]{1,0:T(8,128)(2,1)} async-done(((bf16[8,4096]{1,0:T(8,128)(2,1)}), bf16[128,4096]{1,0:T(8,128)(2,1)}) %all-gather.8.cloned.1.call-update) | async-done | bytes 1048592 | tf_op jit(solution)/shard_map/all_gather | solution.py:59
  90.3 1.5 multiply_reduce_fusion
  91.8 23.9 %all-gather.2 = bf16[16,1,128]{2,1,0:T(2,128)(2,1)S(1)} all-gather(bf16[1,1,128]{2,1,0:T(2,128)(2,1)S(1)} %bitcast.104), channel_id=3, replica_groups=mesh['grp'=2,'sp'=16,'tp'=16] {'sp'}, dimensions={0}, use_global_device_ids=true | all-gather | bytes 4352 | tf_op jit(solution)/shard_map/all_gather | solution.py:94
  115.7 1.3 convolution_convert_fusion.4
  117.1 25.2 %all_gather.20 = bf16[2048,128]{1,0:T(8,128)(2,1)S(1)} all-gather(bf16[128,128]{1,0:T(8,128)(2,1)S(1)} %convolution_convert_fusion.4), channel_id=1, replica_groups=mesh['grp'=2,'sp'=16,'tp'=16] {'sp'}, dimensions={0}, use_global_device_ids=true | all-gather | bytes 557056 | tf_op jit(solution)/shard_map/all_gather | solution.py:89
  142.3 24.2 %all_gather.22 = bf16[2048,128]{0,1:T(8,128)(2,1)S(1)} all-gather(bf16[128,128]{0,1:T(8,128)(2,1)S(1)} %get-tuple-element.8), channel_id=1, replica_groups=mesh['grp'=2,'sp'=16,'tp'=16] {'sp'}, dimensions={0}, use_global_device_ids=true | all-gather | bytes 557056 | tf_op jit(solution)/shard_map/all_gather | solution.py:90
  166.5 3.5 %fusion.17 = bf16[1024,256]{0,1:T(8,128)(2,1)S(1)} fusion(bf16[1024,2048]{1,0:T(8,128)(2,1)} %all-gather.6.cloned.1.call-done, bf16[2048,128]{1,0:T(8,128)(2,1)S(1)} %get-tuple-element.9, bf16[2048,128]{1,0:T(8,128)(2,1)S(1)} %get-tuple-element.10), kind=kOutput, calls=%fused_computation.20 | convolution fusion | flops 1076101120 | bytes 5767168 | tf_op jit(solution)/shard_map/dot_general | solution.py:78
  170.0 1.3 fusion.41
  171.3 2.9 fusion.2
  175.1 1.1 copy-done.2
  176.2 0.9 copy.21
  177.1 7.6 %all-to-all-start = ((bf16[16,128,128]{1,2,0:T(8,128)(2,1)}), bf16[16,128,128]{1,2,0:T(8,128)(2,1)S(1)}, u32[]{:S(2)}, u32[]{:S(2)}) async-start(bf16[16,128,128]{1,2,0:T(8,128)(2,1)} %copy.21), calls=%async_computation | async-start | bytes 1048576 | tf_op jit(solution)/shard_map/all_to_all | solution.py:19
  184.6 3.7 %fusion.27 = bf16[1024,1,128]{0,2,1:T(8,128)(2,1)S(1)} fusion(bf16[2048,128]{1,0:T(8,128)(2,1)S(1)} %all_gather.20, bf16[1024,2048,1]{1,0,2:T(8,128)(2,1)} %copy-done.2), kind=kOutput, calls=%fused_computation.24 | convolution fusion | flops 537001984 | bytes 4980736 | tf_op jit(solution)/shard_map/hnm,nhd->md/dot_general | solution.py:105
  188.4 5.3 %fusion.30 = bf16[1024,1,128]{0,2,1:T(8,128)(2,1)S(1)} fusion(bf16[2048,128]{0,1:T(8,128)(2,1)S(1)} %all_gather.22, f32[1024,2048]{1,0:T(8,128)} %copy-done.1, f32[2048]{0:T(1024)S(1)} %bitcast.102), kind=kOutput, calls=%fused_computation.25 | convolution fusion | flops 545390592 | bytes 9183232 | tf_op jit(solution)/shard_map/hnm,nhd->md/dot_general | solution.py:106
  194.3 1.0 reduce.4
  195.5 0.9 reshape.147
  196.4 4.8 %all-to-all-done = bf16[16,128,128]{1,2,0:T(8,128)(2,1)S(1)} async-done(((bf16[16,128,128]{1,2,0:T(8,128)(2,1)}), bf16[16,128,128]{1,2,0:T(8,128)(2,1)S(1)}, u32[]{:S(2)}, u32[]{:S(2)}) %all-to-all-start) | async-done | bytes 524320 | tf_op jit(solution)/shard_map/all_to_all | solution.py:19
  201.2 25.6 %all-to-all-start.2 = ((bf16[16,2,8192]{2,1,0:T(2,128)(2,1)}), bf16[16,2,8192]{2,1,0:T(2,128)(2,1)S(1)}, u32[]{:S(2)}, u32[]{:S(2)}) async-start(bf16[16,2,8192]{2,1,0:T(2,128)(2,1)} %reshape.147), calls=%async_computation.2 | async-start | bytes 1048576 | tf_op jit(solution)/shard_map/all_to_all | solution.py:115
  226.9 1.1 fusion.16
  228.0 16.0 %all-to-all-done.2 = bf16[16,2,8192]{2,1,0:T(2,128)(2,1)S(1)} async-done(((bf16[16,2,8192]{2,1,0:T(2,128)(2,1)}), bf16[16,2,8192]{2,1,0:T(2,128)(2,1)S(1)}, u32[]{:S(2)}, u32[]{:S(2)}) %all-to-all-start.2) | async-done | bytes 524320 | tf_op jit(solution)/shard_map/all_to_all | solution.py:115
  244.0 3.7 %all-to-all-start.1 = ((bf16[16,8,2048]{2,1,0:T(8,128)(2,1)}), bf16[16,8,2048]{2,1,0:T(8,128)(2,1)S(1)}, u32[]{:S(2)}, u32[]{:S(2)}) async-start(bf16[16,8,2048]{2,1,0:T(8,128)(2,1)} %fusion.16), calls=%async_computation.1 | async-start | bytes 1048576 | tf_op jit(solution)/shard_map/all_to_all | solution.py:19
  247.8 2.2 convolution_convert_fusion
  249.9 14.3 %all-to-all-done.1 = bf16[16,8,2048]{2,1,0:T(8,128)(2,1)S(1)} async-done(((bf16[16,8,2048]{2,1,0:T(8,128)(2,1)}), bf16[16,8,2048]{2,1,0:T(8,128)(2,1)S(1)}, u32[]{:S(2)}, u32[]{:S(2)}) %all-to-all-start.1) | async-done | bytes 524320 | tf_op jit(solution)/shard_map/all_to_all | solution.py:19
  265.0 6.9 %all-to-all-start.3 = ((bf16[16,128,128]{2,1,0:T(8,128)(2,1)}), bf16[16,128,128]{2,1,0:T(8,128)(2,1)}, u32[]{:S(2)}, u32[]{:S(2)}) async-start(bf16[16,128,128]{2,1,0:T(8,128)(2,1)} %bitcast.18), calls=%async_computation.3 | async-start | bytes 1048576 | tf_op jit(solution)/shard_map/all_to_all | solution.py:19
  273.1 2.5 convolution_add_fusion
  275.6 1.1 convert_reduce_fusion.1
  277.6 22.7 %all-to-all-done.3 = bf16[16,128,128]{2,1,0:T(8,128)(2,1)} async-done(((bf16[16,128,128]{2,1,0:T(8,128)(2,1)}), bf16[16,128,128]{2,1,0:T(8,128)(2,1)}, u32[]{:S(2)}, u32[]{:S(2)}) %all-to-all-start.3) | async-done | bytes 524320 | tf_op jit(solution)/shard_map/all_to_all | solution.py:19
  300.2 1.7 convert_reduce_fusion
  (38 shorter events, 7.8 us)
Async XLA Ops:
  7.2 108.5 %copy-start = (bf16[2048,128]{1,0:T(8,128)(2,1)S(1)}, bf16[2048,128]{1,0:T(8,128)(2,1)}, u32[]{:S(2)}) copy-start(bf16[2048,128]{1,0:T(8,128)(2,1)} %param.13) | copy-start | bytes 1572868
  7.2 83.1 %all-gather.8.cloned.1.call-start = ((), (), s32[]{:S(2)}) async-start(), calls=%async_computation.5 | async-start | bytes 1114112 | tf_op jit(solution)/shard_map/all_gather | solution.py:59
  10.5 156.0 %all-gather.6.cloned.1.call-start = ((), (), s32[]{:S(2)}) async-start(), calls=%async_computation.4 | async-start | bytes 4456448 | tf_op jit(solution)/shard_map/all_gather | solution.py:79
  171.2 3.7 %copy-start.1 = (f32[1024,2048]{1,0:T(8,128)}, f32[1024,2048]{1,0:T(8,128)S(1)}, u32[]{:S(2)}) copy-start(f32[1024,2048]{1,0:T(8,128)S(1)} %fusion.41) | copy-start | bytes 25165828
  174.2 2.0 copy-start.2
  177.1 24.1 %all-to-all-start = ((bf16[16,128,128]{1,2,0:T(8,128)(2,1)}), bf16[16,128,128]{1,2,0:T(8,128)(2,1)S(1)}, u32[]{:S(2)}, u32[]{:S(2)}) async-start(bf16[16,128,128]{1,2,0:T(8,128)(2,1)} %copy.21), calls=%async_computation | async-start | bytes 1048576 | tf_op jit(solution)/shard_map/all_to_all | solution.py:19
  193.7 79.0 %copy-start.3 = (bf16[2048,256]{1,0:T(8,128)(2,1)S(1)}, bf16[2048,256]{1,0:T(8,128)(2,1)}, u32[]{:S(2)}) copy-start(bf16[2048,256]{1,0:T(8,128)(2,1)} %param.14) | copy-start | bytes 3145732
  194.3 82.5 %copy-start.5 = (bf16[8,2048]{1,0:T(8,128)(2,1)S(1)}, bf16[8,2048]{1,0:T(8,128)(2,1)}, u32[]{:S(2)}) copy-start(bf16[8,2048]{1,0:T(8,128)(2,1)} %param.10) | copy-start | bytes 98308
  194.3 82.5 %copy-start.6 = (f32[2048]{0:T(1024)S(1)}, f32[2048]{0:T(1024)}, u32[]{:S(2)}) copy-start(f32[2048]{0:T(1024)} %param.12) | copy-start | bytes 24580
  201.2 42.8 %all-to-all-start.2 = ((bf16[16,2,8192]{2,1,0:T(2,128)(2,1)}), bf16[16,2,8192]{2,1,0:T(2,128)(2,1)S(1)}, u32[]{:S(2)}, u32[]{:S(2)}) async-start(bf16[16,2,8192]{2,1,0:T(2,128)(2,1)} %reshape.147), calls=%async_computation.2 | async-start | bytes 1048576 | tf_op jit(solution)/shard_map/all_to_all | solution.py:115
  244.0 20.2 %all-to-all-start.1 = ((bf16[16,8,2048]{2,1,0:T(8,128)(2,1)}), bf16[16,8,2048]{2,1,0:T(8,128)(2,1)S(1)}, u32[]{:S(2)}, u32[]{:S(2)}) async-start(bf16[16,8,2048]{2,1,0:T(8,128)(2,1)} %fusion.16), calls=%async_computation.1 | async-start | bytes 1048576 | tf_op jit(solution)/shard_map/all_to_all | solution.py:19
  264.2 0.8 copy-start.4
  265.0 35.2 %all-to-all-start.3 = ((bf16[16,128,128]{2,1,0:T(8,128)(2,1)}), bf16[16,128,128]{2,1,0:T(8,128)(2,1)}, u32[]{:S(2)}, u32[]{:S(2)}) async-start(bf16[16,128,128]{2,1,0:T(8,128)(2,1)} %bitcast.18), calls=%async_computation.3 | async-start | bytes 1048576 | tf_op jit(solution)/shard_map/all_to_all | solution.py:19
Sparse Core Ops, SparseCore 0:
  10.7 79.5 all-gather.7
  92.4 47.3 all-gather.5
where the time goes:
time: 310 us; the launch traced here: 309 us
  blocking collectives  135 us (44%)
  waiting for transfers between devices  72.8 us (23%)
  starting transfers between devices  43.9 us (14%)
  matrix products  26.5 us (9%)
  between operations  14.3 us (5%)
  other arithmetic  8.82 us (3%)
  local copies, waits for them, and re-layouts  7.37 us (2%)
    all_gather x1, blocking collectives, shards(): lax.all_gather(shift_cols.astype(jnp.bfloat16), 'sp', axis=0, tiled=True)  61.8 us
    all_to_all x3, waiting for transfers between devices, summed_on_arrival(): lax.all_to_all(blocks, axis, split_axis=0, concat_axis=0, tiled=True)  41.7 us
    all_to_all x1, starting transfers between devices, shards(): lax.all_to_all(stacked.astype(jnp.bfloat16), 'tp', split_axis=0, concat_a...  25.6 us
    all_gather x1, blocking collectives, shards(): lax.all_gather(queries, 'sp', axis=0, tiled=True)  25.2 us
    all_gather x1, blocking collectives, shards(): lax.all_gather(out_back, 'sp', axis=0, tiled=True)  24.2 us
    all_gather x1, blocking collectives, shards(): lax.all_gather(drop_cols.astype(jnp.bfloat16), 'sp', axis=0, tiled=True)  23.9 us
    all_to_all x3, starting transfers between devices, summed_on_arrival(): lax.all_to_all(blocks, axis, split_axis=0, concat_axis=0, tiled=True)  18.2 us
    all_to_all x1, waiting for transfers between devices, shards(): lax.all_to_all(stacked.astype(jnp.bfloat16), 'tp', split_axis=0, concat_a...  16 us
  transfers between devices with their start and end apart: 6, of which 5 were waited for; matrix products, arithmetic and copies ran while one was open for 9% of the time, Pallas kernels for 0%

commit v1 on v0

--- a/solution.py
+++ b/solution.py
@@ -86,7 +86,9 @@
     drop_cols = jnp.sum(products.reshape(tgt_local, local_heads, HEAD_DIM), axis=2)
     shift_cols = log_shift.T
     portion = (
-        lax.all_gather(queries, "sp", axis=0, tiled=True),
+        jnp.concatenate(
+            lax.all_to_all(jnp.stack([queries] * lax.axis_size("sp")), "sp", 0, 0), axis=0
+        ),
         lax.all_gather(out_back, "sp", axis=0, tiled=True),
         lax.all_gather(shift_cols.astype(jnp.bfloat16), "sp", axis=0, tiled=True).astype(
             jnp.float32

time: 310 us -> 342 us (1.10)
  waiting for transfers between devices: 72.8 us -> 137 us
  blocking collectives: 135 us -> 85.9 us
  starting transfers between devices: 43.9 us -> 59.1 us
    all_gather x1, waiting for transfers between devices: 14.3 us -> 78.9 us  [shards(): portion = lax.all_gather(joined, 'tp', axis=0, tiled=True)]
    all_gather x1 -> x0, blocking collectives: 25.2 us -> none  [shards(): lax.all_gather(queries, 'sp', axis=0, tiled=True)]
    all_gather x1, blocking collectives: 61.8 us -> 41.3 us  [shards(): lax.all_gather(shift_cols.astype(jnp.bfloat16), 'sp', axis=0, tiled=True)]
    all_to_all x0 -> x1, starting transfers between devices: none -> 12.8 us  [shards(): lax.all_to_all(jnp.stack([queries] * lax.axis_size('sp')), 'sp', 0, 0)]
    all_gather x1, blocking collectives: 23.9 us -> 20.4 us  [shards(): lax.all_gather(drop_cols.astype(jnp.bfloat16), 'sp', axis=0, tiled=True)]
  transfers between devices with their start and end apart: 6 -> 7, of which waited for: 5 -> 5; matrix products, arithmetic and copies ran while one was open for 9% -> 9% of each run, Pallas kernels for 0% -> 0%
where the time goes in v1:
time: 342 us; the launch traced here: 340 us
  waiting for transfers between devices  137 us (40%)
  blocking collectives  85.9 us (25%)
  starting transfers between devices  59.1 us (17%)
  matrix products  26.5 us (8%)
  between operations  14.3 us (4%)
  other arithmetic  8.82 us (3%)
  local copies, waits for them, and re-layouts  8.24 us (2%)
    all_gather x1, waiting for transfers between devices, shards(): portion = lax.all_gather(joined, 'tp', axis=0, tiled=True)  78.9 us
    all_to_all x3, waiting for transfers between devices, summed_on_arrival(): lax.all_to_all(blocks, axis, split_axis=0, concat_axis=0, tiled=True)  41.7 us
    all_gather x1, blocking collectives, shards(): lax.all_gather(shift_cols.astype(jnp.bfloat16), 'sp', axis=0, tiled=True)  41.3 us
    all_to_all x1, starting transfers between devices, shards(): lax.all_to_all(stacked.astype(jnp.bfloat16), 'tp', split_axis=0, concat_a...  26.6 us
    all_gather x1, blocking collectives, shards(): lax.all_gather(out_back, 'sp', axis=0, tiled=True)  24.2 us
    all_gather x1, blocking collectives, shards(): lax.all_gather(drop_cols.astype(jnp.bfloat16), 'sp', axis=0, tiled=True)  20.4 us
    all_to_all x3, starting transfers between devices, summed_on_arrival(): lax.all_to_all(blocks, axis, split_axis=0, concat_axis=0, tiled=True)  19.6 us
    all_to_all x1, waiting for transfers between devices, shards(): lax.all_to_all(stacked.astype(jnp.bfloat16), 'tp', split_axis=0, concat_a...  16 us
  transfers between devices with their start and end apart: 7, of which 5 were waited for; matrix products, arithmetic and copies ran while one was open for 9% of the time, Pallas kernels for 0%

profile of v1, /device:TPU:65, one launch (start us, length us, event | category | flops | bytes accessed | tf_op | source)
XLA Modules:
  0.0 340.3 jit_solution(14935696180453917850)
XLA Ops:
  7.3 0.9 fusion.43
  9.1 1.4 pad_maximum_fusion.1
  11.3 78.9 %all-gather.8.cloned.1.call-done = bf16[128,4096]{1,0:T(8,128)(2,1)} async-done(((bf16[8,4096]{1,0:T(8,128)(2,1)}), bf16[128,4096]{1,0:T(8,128)(2,1)}) %all-gather.8.cloned.1.call-update) | async-done | bytes 1048592 | tf_op jit(solution)/shard_map/all_gather | solution.py:59
  90.2 1.3 convolution_convert_fusion.4
  92.5 12.8 %all-to-all-start = ((bf16[16,128,128]{2,1,0:T(8,128)(2,1)}), bf16[16,128,128]{2,1,0:T(8,128)(2,1)S(1)}, u32[]{:S(2)}, u32[]{:S(2)}) async-start(bf16[16,128,128]{2,1,0:T(8,128)(2,1)} %stack.2), calls=%async_computation | async-start | bytes 1048576 | tf_op jit(solution)/shard_map/all_to_all | solution.py:90
  106.8 41.3 %all-gather = bf16[1,2048]{1,0:T(2,128)(2,1)S(1)} all-gather(bf16[1,128]{1,0:T(2,128)(2,1)S(1)} %convert_element_type.126), channel_id=2, replica_groups=mesh['grp'=2,'sp'=16,'tp'=16] {'sp'}, dimensions={1}, use_global_device_ids=true | all-gather | bytes 4352 | tf_op jit(solution)/shard_map/all_gather | solution.py:93
  148.2 1.3 constant_dynamic-slice_fusion
  149.5 1.5 multiply_reduce_fusion
  151.0 20.4 %all-gather.2 = bf16[16,1,128]{2,1,0:T(2,128)(2,1)S(1)} all-gather(bf16[1,1,128]{2,1,0:T(2,128)(2,1)S(1)} %bitcast.107), channel_id=3, replica_groups=mesh['grp'=2,'sp'=16,'tp'=16] {'sp'}, dimensions={0}, use_global_device_ids=true | all-gather | bytes 4352 | tf_op jit(solution)/shard_map/all_gather | solution.py:96
  171.3 24.2 %all_gather.18 = bf16[2048,128]{0,1:T(8,128)(2,1)S(1)} all-gather(bf16[128,128]{0,1:T(8,128)(2,1)S(1)} %get-tuple-element.8), channel_id=1, replica_groups=mesh['grp'=2,'sp'=16,'tp'=16] {'sp'}, dimensions={0}, use_global_device_ids=true | all-gather | bytes 557056 | tf_op jit(solution)/shard_map/all_gather | solution.py:92
  195.6 3.5 %fusion.17 = bf16[1024,256]{0,1:T(8,128)(2,1)S(1)} fusion(bf16[1024,2048]{1,0:T(8,128)(2,1)} %all-gather.6.cloned.1.call-done, bf16[2048,128]{1,0:T(8,128)(2,1)S(1)} %get-tuple-element.9, bf16[2048,128]{1,0:T(8,128)(2,1)S(1)} %get-tuple-element.10), kind=kOutput, calls=%fused_computation.20 | convolution fusion | flops 1076101120 | bytes 5767168 | tf_op jit(solution)/shard_map/dot_general | solution.py:78
  199.1 1.3 fusion.41
  200.4 2.9 fusion.2
  204.2 1.1 copy-done.2
  205.2 0.9 copy.21
  206.2 9.0 %all-to-all-start.1 = ((bf16[16,128,128]{1,2,0:T(8,128)(2,1)}), bf16[16,128,128]{1,2,0:T(8,128)(2,1)S(1)}, u32[]{:S(2)}, u32[]{:S(2)}) async-start(bf16[16,128,128]{1,2,0:T(8,128)(2,1)} %copy.21), calls=%async_computation.1 | async-start | bytes 1048576 | tf_op jit(solution)/shard_map/all_to_all | solution.py:19
  215.1 3.7 %fusion.27 = bf16[1024,1,128]{0,2,1:T(8,128)(2,1)S(1)} fusion(bf16[2048,128]{1,0:T(8,128)(2,1)S(1)} %bitcast.101, bf16[1024,2048,1]{1,0,2:T(8,128)(2,1)} %copy-done.2), kind=kOutput, calls=%fused_computation.24 | convolution fusion | flops 537001984 | bytes 4980736 | tf_op jit(solution)/shard_map/hnm,nhd->md/dot_general | solution.py:107
  218.8 5.3 %fusion.30 = bf16[1024,1,128]{0,2,1:T(8,128)(2,1)S(1)} fusion(bf16[2048,128]{0,1:T(8,128)(2,1)S(1)} %all_gather.18, f32[1024,2048]{1,0:T(8,128)} %copy-done.1, f32[2048]{0:T(1024)S(1)} %bitcast.105), kind=kOutput, calls=%fused_computation.25 | convolution fusion | flops 545390592 | bytes 9183232 | tf_op jit(solution)/shard_map/hnm,nhd->md/dot_general | solution.py:108
  224.7 1.0 reduce.4
  226.0 0.9 reshape.151
  226.9 4.8 %all-to-all-done.1 = bf16[16,128,128]{1,2,0:T(8,128)(2,1)S(1)} async-done(((bf16[16,128,128]{1,2,0:T(8,128)(2,1)}), bf16[16,128,128]{1,2,0:T(8,128)(2,1)S(1)}, u32[]{:S(2)}, u32[]{:S(2)}) %all-to-all-start.1) | async-done | bytes 524320 | tf_op jit(solution)/shard_map/all_to_all | solution.py:19
  231.7 26.6 %all-to-all-start.3 = ((bf16[16,2,8192]{2,1,0:T(2,128)(2,1)}), bf16[16,2,8192]{2,1,0:T(2,128)(2,1)S(1)}, u32[]{:S(2)}, u32[]{:S(2)}) async-start(bf16[16,2,8192]{2,1,0:T(2,128)(2,1)} %reshape.151), calls=%async_computation.3 | async-start | bytes 1048576 | tf_op jit(solution)/shard_map/all_to_all | solution.py:117
  258.3 1.1 fusion.16
  259.5 16.0 %all-to-all-done.3 = bf16[16,2,8192]{2,1,0:T(2,128)(2,1)S(1)} async-done(((bf16[16,2,8192]{2,1,0:T(2,128)(2,1)}), bf16[16,2,8192]{2,1,0:T(2,128)(2,1)S(1)}, u32[]{:S(2)}, u32[]{:S(2)}) %all-to-all-start.3) | async-done | bytes 524320 | tf_op jit(solution)/shard_map/all_to_all | solution.py:117
  275.5 3.7 %all-to-all-start.2 = ((bf16[16,8,2048]{2,1,0:T(8,128)(2,1)}), bf16[16,8,2048]{2,1,0:T(8,128)(2,1)S(1)}, u32[]{:S(2)}, u32[]{:S(2)}) async-start(bf16[16,8,2048]{2,1,0:T(8,128)(2,1)} %fusion.16), calls=%async_computation.2 | async-start | bytes 1048576 | tf_op jit(solution)/shard_map/all_to_all | solution.py:19
  279.2 2.2 convolution_convert_fusion
  281.4 14.3 %all-to-all-done.2 = bf16[16,8,2048]{2,1,0:T(8,128)(2,1)S(1)} async-done(((bf16[16,8,2048]{2,1,0:T(8,128)(2,1)}), bf16[16,8,2048]{2,1,0:T(8,128)(2,1)S(1)}, u32[]{:S(2)}, u32[]{:S(2)}) %all-to-all-start.2) | async-done | bytes 524320 | tf_op jit(solution)/shard_map/all_to_all | solution.py:19
  296.5 6.9 %all-to-all-start.4 = ((bf16[16,128,128]{2,1,0:T(8,128)(2,1)}), bf16[16,128,128]{2,1,0:T(8,128)(2,1)}, u32[]{:S(2)}, u32[]{:S(2)}) async-start(bf16[16,128,128]{2,1,0:T(8,128)(2,1)} %bitcast.19), calls=%async_computation.4 | async-start | bytes 1048576 | tf_op jit(solution)/shard_map/all_to_all | solution.py:19
  304.6 2.5 convolution_add_fusion
  307.0 1.1 convert_reduce_fusion.1
  309.0 22.7 %all-to-all-done.4 = bf16[16,128,128]{2,1,0:T(8,128)(2,1)} async-done(((bf16[16,128,128]{2,1,0:T(8,128)(2,1)}), bf16[16,128,128]{2,1,0:T(8,128)(2,1)}, u32[]{:S(2)}, u32[]{:S(2)}) %all-to-all-start.4) | async-done | bytes 524320 | tf_op jit(solution)/shard_map/all_to_all | solution.py:19
  331.7 1.7 convert_reduce_fusion
  (40 shorter events, 8.7 us)
Async XLA Ops:
  7.2 83.1 %copy-start = (bf16[2048,128]{1,0:T(8,128)(2,1)S(1)}, bf16[2048,128]{1,0:T(8,128)(2,1)}, u32[]{:S(2)}) copy-start(bf16[2048,128]{1,0:T(8,128)(2,1)} %param.13) | copy-start | bytes 1572868
  7.2 83.0 %all-gather.8.cloned.1.call-start = ((), (), s32[]{:S(2)}) async-start(), calls=%async_computation.6 | async-start | bytes 1114112 | tf_op jit(solution)/shard_map/all_gather | solution.py:59
  10.5 185.1 %all-gather.6.cloned.1.call-start = ((), (), s32[]{:S(2)}) async-start(), calls=%async_computation.5 | async-start | bytes 4456448 | tf_op jit(solution)/shard_map/all_gather | solution.py:79
  92.5 106.6 %all-to-all-start = ((bf16[16,128,128]{2,1,0:T(8,128)(2,1)}), bf16[16,128,128]{2,1,0:T(8,128)(2,1)S(1)}, u32[]{:S(2)}, u32[]{:S(2)}) async-start(bf16[16,128,128]{2,1,0:T(8,128)(2,1)} %stack.2), calls=%async_computation | async-start | bytes 1048576 | tf_op jit(solution)/shard_map/all_to_all | solution.py:90
  200.4 3.7 %copy-start.1 = (f32[1024,2048]{1,0:T(8,128)}, f32[1024,2048]{1,0:T(8,128)S(1)}, u32[]{:S(2)}) copy-start(f32[1024,2048]{1,0:T(8,128)S(1)} %fusion.41) | copy-start | bytes 25165828
  203.3 1.9 copy-start.2
  206.2 25.5 %all-to-all-start.1 = ((bf16[16,128,128]{1,2,0:T(8,128)(2,1)}), bf16[16,128,128]{1,2,0:T(8,128)(2,1)S(1)}, u32[]{:S(2)}, u32[]{:S(2)}) async-start(bf16[16,128,128]{1,2,0:T(8,128)(2,1)} %copy.21), calls=%async_computation.1 | async-start | bytes 1048576 | tf_op jit(solution)/shard_map/all_to_all | solution.py:19
  224.2 80.0 %copy-start.3 = (bf16[2048,256]{1,0:T(8,128)(2,1)S(1)}, bf16[2048,256]{1,0:T(8,128)(2,1)}, u32[]{:S(2)}) copy-start(bf16[2048,256]{1,0:T(8,128)(2,1)} %param.14) | copy-start | bytes 3145732
  224.7 83.4 %copy-start.5 = (bf16[8,2048]{1,0:T(8,128)(2,1)S(1)}, bf16[8,2048]{1,0:T(8,128)(2,1)}, u32[]{:S(2)}) copy-start(bf16[8,2048]{1,0:T(8,128)(2,1)} %param.10) | copy-start | bytes 98308
  224.7 83.4 %copy-start.6 = (f32[2048]{0:T(1024)S(1)}, f32[2048]{0:T(1024)}, u32[]{:S(2)}) copy-start(f32[2048]{0:T(1024)} %param.12) | copy-start | bytes 24580
  231.7 43.8 %all-to-all-start.3 = ((bf16[16,2,8192]{2,1,0:T(2,128)(2,1)}), bf16[16,2,8192]{2,1,0:T(2,128)(2,1)S(1)}, u32[]{:S(2)}, u32[]{:S(2)}) async-start(bf16[16,2,8192]{2,1,0:T(2,128)(2,1)} %reshape.151), calls=%async_computation.3 | async-start | bytes 1048576 | tf_op jit(solution)/shard_map/all_to_all | solution.py:117
  275.5 20.2 %all-to-all-start.2 = ((bf16[16,8,2048]{2,1,0:T(8,128)(2,1)}), bf16[16,8,2048]{2,1,0:T(8,128)(2,1)S(1)}, u32[]{:S(2)}, u32[]{:S(2)}) async-start(bf16[16,8,2048]{2,1,0:T(8,128)(2,1)} %fusion.16), calls=%async_computation.2 | async-start | bytes 1048576 | tf_op jit(solution)/shard_map/all_to_all | solution.py:19
  295.7 0.8 copy-start.4
  296.5 35.2 %all-to-all-start.4 = ((bf16[16,128,128]{2,1,0:T(8,128)(2,1)}), bf16[16,128,128]{2,1,0:T(8,128)(2,1)}, u32[]{:S(2)}, u32[]{:S(2)}) async-start(bf16[16,128,128]{2,1,0:T(8,128)(2,1)} %bitcast.19), calls=%async_computation.4 | async-start | bytes 1048576 | tf_op jit(solution)/shard_map/all_to_all | solution.py:19
Sparse Core Ops, SparseCore 0:
  10.7 79.4 all-gather.7
  92.4 47.4 all-gather.5
